TPU v7x, 32 devices: a whole 2x2x4 slice. The times are simulated.
32 devices in a mesh: fs: 4 (over z), tp: 8 (over y, x, core).
Axes of the slice: x: 2, y: 2, z: 4, core: 2. Of those that a mesh axis runs over, the one named last changes fastest.
Arguments:
- inputs: bfloat16 [1024, 2016], P('fs'), may hold values from -6 to 6
- pre_act: bfloat16 [1024, 4032], P('fs', 'tp'), may hold values from -6 to 6
- cotangent: bfloat16 [1024, 2016], P('fs'), may hold values from -6 to 6
- w_up: bfloat16 [2016, 4032], P('fs', 'tp'), may hold values from -0.125 to 0.125
- w_down: bfloat16 [4032, 2016], P('tp', 'fs'), may hold values from -0.09375 to 0.09375
Outputs:
- grad_input: bfloat16 [1024, 2016], P('fs')
- grad_up: float32 [2016, 4032], P('fs', 'tp')
- grad_down: float32 [4032, 2016], P('tp', 'fs')
All inputs are finite; a program needn't handle non-finite values.
Results may differ from a plain program's by a relative error of at most 0.017.
Values may be sent and summed in bfloat16 or wider, within the bound.
A program may use at most 64 MiB of HBM per device.

v0:
```python
import jax
import jax.numpy as jnp
from jax import lax
from jax.sharding import PartitionSpec as P


def on_device(inputs, pre_act, cotangent, w_up, w_down):
    positive = jnp.maximum(pre_act.astype(jnp.float32), 0.0)
    hidden = (positive * positive).astype(jnp.bfloat16)
    columns = cotangent
    hidden_grad = lax.dot_general(
        columns,
        lax.all_gather(w_down, "fs", axis=1, tiled=True),
        (((1,), (1,)), ((), ())),
        preferred_element_type=jnp.float32,
    )
    pre_grad = (2.0 * positive * hidden_grad).astype(jnp.bfloat16)
    columns = inputs
    grad_up = lax.psum_scatter(
        lax.dot_general(
            columns, pre_grad, (((0,), (0,)), ((), ())), preferred_element_type=jnp.float32
        ).astype(jnp.bfloat16),
        "fs",
        scatter_dimension=0,
        tiled=True,
    ).astype(jnp.float32)
    columns = cotangent
    grad_down = (
        lax.psum_scatter(
            lax.dot_general(
                columns, hidden, (((0,), (0,)), ((), ())), preferred_element_type=jnp.float32
            ).astype(jnp.bfloat16),
            "fs",
            scatter_dimension=0,
            tiled=True,
        )
        .astype(jnp.float32)
        .T
    )
    partial_sum = lax.dot_general(
        pre_grad,
        lax.all_gather(w_up, "fs", axis=0, tiled=True),
        (((1,), (1,)), ((), ())),
        preferred_element_type=jnp.float32,
    ).astype(jnp.bfloat16)
    shares = (
        lax.psum_scatter(partial_sum, "tp", scatter_dimension=0, tiled=True)
        .astype(jnp.float32)
        .astype(jnp.bfloat16)
    )
    grad_input = lax.all_gather(shares, "tp", axis=0, tiled=True)
    return (grad_input, grad_up, grad_down)


def solution(mesh):
    in_specs = (P("fs", None), P("fs", "tp"), P("fs", None), P("fs", "tp"), P("tp", "fs"))
    out_specs = (P("fs", None), P("fs", "tp"), P("tp", "fs"))
    return jax.shard_map(
        on_device, mesh=mesh, in_specs=in_specs, out_specs=out_specs, check_vma=False
    )
```

profile of v0, /device:TPU:0, one launch (start us, length us, event | category | flops | bytes accessed | tf_op | source)
XLA Modules:
  0.0 240.3 jit_solution(424361379312722915)
XLA Ops:
  7.2 0.0 copy-start
  7.2 0.0 copy-start.1
  7.2 0.0 all-gather.3.cloned.1.call-start
  7.2 2.1 copy.10
  9.4 0.0 all-gather.3.cloned.1.call-update
  9.4 0.0 all-gather.5.cloned.1.call-start
  9.4 0.7 all-gather.5.cloned.1.call-update
  10.1 0.0 reduce-scatter.12.cloned.1.call-start
  10.2 0.0 copy-done
  10.2 0.0 copy-done.1
  10.2 0.7 fusion.1
  11.0 2.4 %copy.15 = bf16[2016,504]{1,0:T(8,128)(2,1)} copy(bf16[2016,504]{0,1:T(8,128)(2,1)S(1)} %fusion.1) | data formatting | bytes 4064256
  13.4 0.0 reduce-scatter.12.cloned.1.call-update
  13.4 0.0 reduce-scatter.8.cloned.1.call-start
  13.5 44.5 %all-gather.3.cloned.1.call-done = bf16[504,2016]{0,1:T(8,128)(2,1)} async-done(((bf16[504,504]{0,1:T(8,128)(2,1)}), bf16[504,2016]{0,1:T(8,128)(2,1)}) %all-gather.3.cloned.1.call-update) | async-done | bytes 2032144 | tf_op jit(solution)/shard_map/all_gather | solution.py:13
  58.0 2.5 %fusion.2 = bf16[256,504]{0,1:T(8,128)(2,1)S(1)} fusion(bf16[256,2016]{0,1:T(8,128)(2,1)S(1)} %copy-done, bf16[504,2016]{0,1:T(8,128)(2,1)} %all-gather.3.cloned.1.call-done, bf16[256,504]{0,1:T(8,128)(2,1)S(1)} %copy-done.1), kind=kOutput, calls=%fused_computation.6 | convolution fusion | flops 520869888 | bytes 3580416 | tf_op jit(solution)/shard_map/dot_general | solution.py:11
  60.5 43.0 %all-gather.5.cloned.1.call-done = bf16[2016,504]{1,0:T(8,128)(2,1)} async-done(((bf16[504,504]{1,0:T(8,128)(2,1)}), bf16[2016,504]{1,0:T(8,128)(2,1)}) %all-gather.5.cloned.1.call-update) | async-done | bytes 2032144 | tf_op jit(solution)/shard_map/all_gather | solution.py:42
  103.5 3.3 %convolution_convert_fusion.2 = bf16[256,2016]{1,0:T(8,128)(2,1)} fusion(bf16[256,504]{0,1:T(8,128)(2,1)S(1)} %fusion.2, bf16[2016,504]{1,0:T(8,128)(2,1)} %all-gather.5.cloned.1.call-done), kind=kOutput, calls=%fused_computation.4 | convolution fusion | flops 520740864 | bytes 3322368 | tf_op jit(solution)/shard_map/dot_general | solution.py:40
  106.9 0.0 reduce-scatter.8.cloned.1.call-update
  106.9 0.0 reduce-scatter.10.cloned.1.call-start
  106.9 2.0 fusion
  108.9 2.4 %copy.13 = bf16[2016,504]{1,0:T(8,128)(2,1)} copy(bf16[2016,504]{0,1:T(8,128)(2,1)S(1)} %fusion) | data formatting | bytes 4064256
  111.3 0.0 reduce-scatter.10.cloned.1.call-update
  111.4 36.5 %reduce-scatter.12.cloned.1.call-done = bf16[504,504]{1,0:T(8,128)(2,1)} async-done(((bf16[2016,504]{1,0:T(8,128)(2,1)}), bf16[504,504]{1,0:T(8,128)(2,1)}) %reduce-scatter.12.cloned.1.call-update) | async-done | bytes 508048
  147.9 1.2 copy.16
  149.1 1.1 convert_bitcast_fusion
  150.2 35.9 %reduce-scatter.8.cloned.1.call-done = bf16[32,2016]{1,0:T(8,128)(2,1)} async-done(((bf16[256,2016]{1,0:T(8,128)(2,1)}), bf16[32,2016]{1,0:T(8,128)(2,1)}) %reduce-scatter.8.cloned.1.call-update) | async-done | bytes 129040 | tf_op jit(solution)/shard_map/reduce_scatter | solution.py:47
  186.1 10.9 %all_gather.11 = bf16[256,2016]{1,0:T(8,128)(2,1)S(1)} all-gather(bf16[32,2016]{1,0:T(8,128)(2,1)} %reduce-scatter.8.cloned.1.call-done), channel_id=1, replica_groups=mesh['fs'=4,'tp'=8] {'tp'}, dimensions={0}, use_global_device_ids=true | all-gather | bytes 1161216 | tf_op jit(solution)/shard_map/all_gather | solution.py:51
  197.0 1.3 copy.11
  198.3 33.1 %reduce-scatter.10.cloned.1.call-done = bf16[504,504]{1,0:T(8,128)(2,1)} async-done(((bf16[2016,504]{1,0:T(8,128)(2,1)}), bf16[504,504]{1,0:T(8,128)(2,1)}) %reduce-scatter.10.cloned.1.call-update) | async-done | bytes 508048
  231.4 1.2 copy.14
  232.6 1.2 copy.12
Async XLA Ops:
  7.2 3.0 %copy-start = (bf16[256,2016]{0,1:T(8,128)(2,1)S(1)}, bf16[256,2016]{0,1:T(8,128)(2,1)}, u32[]{:S(2)}) copy-start(bf16[256,2016]{0,1:T(8,128)(2,1)} %param.7) | copy-start | bytes 3096580
  7.2 3.0 %copy-start.1 = (bf16[256,504]{0,1:T(8,128)(2,1)S(1)}, bf16[256,504]{0,1:T(8,128)(2,1)}, u32[]{:S(2)}) copy-start(bf16[256,504]{0,1:T(8,128)(2,1)} %param.6) | copy-start | bytes 774148
  7.2 50.8 %all-gather.3.cloned.1.call-start = ((), (), s32[]{:S(2)}) async-start(), calls=%async_computation.3 | async-start | bytes 2580480 | tf_op jit(solution)/shard_map/all_gather | solution.py:13
  9.4 94.2 %all-gather.5.cloned.1.call-start = ((), (), s32[]{:S(2)}) async-start(), calls=%async_computation.4 | async-start | bytes 2580480 | tf_op jit(solution)/shard_map/all_gather | solution.py:42
  10.1 137.7 %reduce-scatter.12.cloned.1.call-start = ((), (), s32[]{:S(2)}) async-start(), calls=%async_computation.7 | async-start | bytes 2580480
  13.4 172.6 %reduce-scatter.8.cloned.1.call-start = ((), (), s32[]{:S(2)}) async-start(), calls=%async_computation.5 | async-start | bytes 1179648 | tf_op jit(solution)/shard_map/reduce_scatter | solution.py:47
  106.9 124.5 %reduce-scatter.10.cloned.1.call-start = ((), (), s32[]{:S(2)}) async-start(), calls=%async_computation.6 | async-start | bytes 2580480
Sparse Core Ops, SparseCore 0:
  10.1 47.8 all-gather.2
  59.6 43.9 all-gather.4
  105.9 41.9 reduce-scatter.11
  150.9 35.1 reduce-scatter.7
  188.2 43.0 reduce-scatter.9
where the time goes:
time: 241 us; the launch traced here: 240 us
  waiting for transfers between devices  194 us (80%)
  between operations  13.8 us (6%)
  local copies, waits for them, and re-layouts  12 us (5%)
  blocking collectives  10.9 us (5%)
  matrix products  8.52 us (4%)
    unnamed x7, waiting for transfers between devices  70.4 us
    all_gather x1, waiting for transfers between devices, on_device(): lax.all_gather(w_down, 'fs', axis=1, tiled=True)  44.5 us
    all_gather x1, waiting for transfers between devices, on_device(): lax.all_gather(w_up, 'fs', axis=0, tiled=True)  43 us
    reduce_scatter x1, waiting for transfers between devices, on_device(): lax.psum_scatter(partial_sum, 'tp', scatter_dimension=0, tiled=True)  35.9 us
    unnamed x11, local copies, waits for them, and re-layouts  12 us
    all_gather x1, blocking collectives, on_device(): grad_input = lax.all_gather(shares, 'tp', axis=0, tiled=True)  10.9 us
  transfers between devices with their start and end apart: 5, of which 5 were waited for; matrix products, arithmetic and copies ran while one was open for 7% of the time, Pallas kernels for 0%

commit v1 on v0

--- a/solution.py
+++ b/solution.py
@@ -1,7 +1,297 @@
+import functools
+
 import jax
 import jax.numpy as jnp
 from jax import lax
+from jax.experimental import pallas as pl
+from jax.experimental.pallas import tpu as pltpu
 from jax.sharding import PartitionSpec as P
+
+MESH = pl.DeviceIdType.MESH
+F32 = jnp.float32
+BF16 = jnp.bfloat16
+NT = (((1,), (1,)), ((), ()))
+TN = (((0,), (0,)), ((), ()))
+
+
+def kernel(nf, nt, pieces, inputs, pre_act, cotangent, w_up, w_down, grad_input, grad_up, grad_down,
+           cot_split, in_split, cot_all, in_all, pa, pg, hg, rs_out, rs_in, px_out, px_in, keep,
+           xy_out, xy_in, zt_out, share,
+           a2a_s, a2a_r, ring_s, ring_r, pair_s, pair_r, rs_s, rs_r, ag_s, ag_r,
+           px_s, px_r, xy_s, xy_r, zt_s, zt_r, fa_s, fa_r, fd_s, fd_r):
+    f, t = lax.axis_index("fs"), lax.axis_index("tp")
+    half = nt // 2
+    rows, width = pre_act.shape
+    part = rows // nt
+    block = w_up.shape[0]
+    step_rows = rows // pieces
+    odd = lax.rem(t, 2)
+    partner = t + 1 - 2 * odd
+    sent = []
+
+    def copy(src, dst, ssem, rsem, fs=None, tp=None):
+        return pltpu.make_async_remote_copy(
+            src_ref=src, dst_ref=dst, send_sem=ssem, recv_sem=rsem,
+            device_id=(f if fs is None else fs, t if tp is None else tp), device_id_type=MESH,
+        )
+
+    def start(desc, cond=None):
+        sent.append((cond, desc))
+        if cond is None:
+            desc.start()
+        else:
+            pl.when(cond)(desc.start)
+
+    def peer(i):
+        return lax.rem(t + 2 * i, nt)
+
+    def source(i):
+        return lax.rem(t + nt - 2 * i, nt)
+
+    barrier = pltpu.get_barrier_semaphore()
+    for off in range(1, nf):
+        pl.semaphore_signal(barrier, inc=1, device_id=(lax.rem(f + off, nf), t), device_id_type=MESH)
+    for i in range(1, half):
+        pl.semaphore_signal(barrier, inc=1, device_id=(f, peer(i)), device_id_type=MESH)
+    pl.semaphore_signal(barrier, inc=1, device_id=(f, partner), device_id_type=MESH)
+
+    def split(src, dst):
+        for g in range(nf):
+            dst[g] = src[:, g * block:(g + 1) * block].reshape(nt, part, block)
+
+    split(cotangent, cot_split)
+    pl.semaphore_wait(barrier, nf - 1 + half)
+
+    def exchange(n, src, dst):
+        for off in range(nf - 1, 0, -1):
+            g = lax.rem(f + off, nf)
+            start(copy(src.at[g, t], dst.at[f, t], a2a_s.at[n, off], a2a_r.at[n, off], fs=g))
+
+    def spread(n, src, dst):
+        for off in range(1, nf):
+            g = lax.rem(f + nf - off, nf)
+            copy(src.at[g, t], dst.at[g, t], a2a_s.at[n, off], a2a_r.at[n, off], fs=g).wait_recv()
+            for i in range(1, half):
+                start(copy(dst.at[g, t], dst.at[g, t], ring_s.at[n, off, i], ring_r.at[n, off, i], tp=peer(i)))
+            start(copy(dst.at[g, t], dst.at[g, t], pair_s.at[n, off, 0], pair_r.at[n, off, 0], tp=partner))
+
+    def relay(n, dst):
+        for off in range(1, nf):
+            g = lax.rem(f + nf - off, nf)
+            for i in range(1, half):
+                at = dst.at[g, source(i)]
+                copy(at, at, ring_s.at[n, off, i], ring_r.at[n, off, i], tp=source(i)).wait_recv()
+                start(copy(at, at, pair_s.at[n, off, i], pair_r.at[n, off, i], tp=partner))
+
+    def collect(n, dst):
+        for off in range(1, nf):
+            g = lax.rem(f + nf - off, nf)
+            for i in range(half):
+                at = dst.at[g, lax.rem(partner + nt - 2 * i, nt)]
+                copy(at, at, pair_s.at[n, off, i], pair_r.at[n, off, i], tp=partner).wait_recv()
+
+    def nearest(m):
+        a = jnp.minimum(f, nf - 1 - f)
+        j = (m - 1) // 2
+        near = f - 1 - j if m % 2 == 1 else f + 1 + j
+        far = jnp.where(f < nf - 1 - f, f + (m - a), f - (m - a))
+        return jnp.where(m <= 2 * a, near, far)
+
+    def gather_own(n, buf, s, size):
+        at = buf.at[f, pl.ds(s * size, size)]
+        start(copy(at, at, ag_s.at[n, 0, 0, s], ag_r.at[n, 0, 0, s], fs=jnp.minimum(f + 1, nf - 1)), f < nf - 1)
+        start(copy(at, at, ag_s.at[n, 1, 0, s], ag_r.at[n, 1, 0, s], fs=jnp.maximum(f - 1, 0)), f > 0)
+
+    def gather_next(n, buf, m, s, size):
+        g = nearest(m)
+        up = g < f
+        d = jnp.where(up, 0, 1)
+        j = jnp.abs(g - f) - 1
+        at = buf.at[g, pl.ds(s * size, size)]
+        copy(at, at, ag_s.at[n, d, j, s], ag_r.at[n, d, j, s], fs=jnp.where(up, f - 1, f + 1)).wait_recv()
+        to = jnp.where(up, f + 1, f - 1)
+        cond = jnp.logical_and(to >= 0, to < nf)
+        to = jnp.clip(to, 0, nf - 1)
+        k = jnp.minimum(j + 1, nf - 1)
+        start(copy(at, at, ag_s.at[n, d, k, s], ag_r.at[n, d, k, s], fs=to), cond)
+
+    exchange(0, cot_split, cot_all)
+    pa[f] = pre_act[...]
+    gather_own(0, pa, 0, rows)
+    split(inputs, in_split)
+    cot_all[f] = cot_split[f]
+    in_all[f] = in_split[f]
+    spread(0, cot_split, cot_all)
+    exchange(1, in_split, in_all)
+    relay(0, cot_all)
+    collect(0, cot_all)
+
+    for g in range(nf):
+        hg[g] = lax.dot_general(cot_all[g].reshape(rows, block), w_down[...], NT, preferred_element_type=F32)
+
+    def reduce_step(s, d, g):
+        at = pl.ds(s * step_rows, step_rows)
+        lower = d == 0
+        first = f == 0 if lower else f == nf - 1
+        passes = g > f if lower else g < f
+        ends = f == g
+        to = jnp.minimum(f + 1, nf - 1) if lower else jnp.maximum(f - 1, 0)
+        back = jnp.maximum(f - 1, 0) if lower else jnp.minimum(f + 1, nf - 1)
+        out = rs_out.at[d, g, at]
+        into = rs_in.at[d, g, at]
+        arrives = jnp.logical_and(jnp.logical_not(first), jnp.logical_or(passes, ends))
+
+        @pl.when(arrives)
+        def _():
+            copy(out, into, rs_s.at[d, g, s], rs_r.at[d, g, s], fs=back).wait_recv()
+            hg[g, at] = hg[g, at] + rs_in[d, g, at].astype(F32)
+
+        @pl.when(passes)
+        def _():
+            rs_out[d, g, at] = hg[g, at].astype(BF16)
+
+        start(copy(out, into, rs_s.at[d, g, s], rs_r.at[d, g, s], fs=to), passes)
+
+    for s in range(pieces):
+        for k in range(nf):
+            reduce_step(s, 0, nf - 1 - k)
+            reduce_step(s, 1, k)
+        at = pl.ds(s * step_rows, step_rows)
+        positive = jnp.maximum(pre_act[at, :].astype(F32), 0.0)
+        pg[f, at] = (2.0 * positive * hg[f, at]).astype(BF16)
+        gather_own(1, pg, s, step_rows)
+        if s == 0:
+            gather_next(0, pa, 1, 0, rows)
+            spread(1, in_split, in_all)
+    for m in range(2, nf):
+        gather_next(0, pa, m, 0, rows)
+
+    def term(step, g):
+        value = lax.dot_general(pg[g], w_up[...], NT, preferred_element_type=F32).astype(BF16)
+        value = value.reshape(half, 2, part, block)
+
+        @pl.when(odd == 0)
+        def _():
+            keep[step] = value[:, 0]
+            px_out[step] = value[:, 1]
+
+        @pl.when(odd == 1)
+        def _():
+            keep[step] = value[:, 1]
+            px_out[step] = value[:, 0]
+
+        start(copy(px_out.at[step], px_in.at[step], px_s.at[step], px_r.at[step], tp=partner))
+
+    def pair_sum(step):
+        copy(px_out.at[step], px_in.at[step], px_s.at[step], px_r.at[step], tp=partner).wait_recv()
+        xy_out[step] = (keep[step].astype(F32) + px_in[step].astype(F32)).astype(BF16)
+        for i in range(1, half):
+            start(copy(xy_out.at[step, lax.rem(t // 2 + i, half)], xy_in.at[step, i],
+                       xy_s.at[step, i], xy_r.at[step, i], tp=peer(i)))
+
+    def finish(step, g):
+        mine = t // 2
+        total = keep[step, mine].astype(F32) + px_in[step, mine].astype(F32)
+        for i in range(1, half):
+            copy(xy_in.at[step, i], xy_in.at[step, i], xy_s.at[step, i], xy_r.at[step, i], tp=source(i)).wait_recv()
+            total = total + xy_in[step, i].astype(F32)
+        if step == 0:
+            share[t, f] = total.astype(BF16)
+        else:
+            zt_out[step] = total.astype(BF16)
+            off = lax.rem(g - f + nf, nf)
+            start(copy(zt_out.at[step], share.at[t, f], zt_s.at[off], zt_r.at[off], fs=g))
+
+    order = [f] + [nearest(m) for m in range(1, nf)]
+    term(0, f)
+    pair_sum(0)
+    relay(1, in_all)
+    tokens = nf * rows
+    for m in range(1, nf):
+        for s in range(pieces):
+            gather_next(1, pg, m, s, step_rows)
+        term(m, order[m])
+        pair_sum(m)
+        if m == 1:
+            positive = jnp.maximum(pa[...].reshape(tokens, width).astype(F32), 0.0)
+            hidden = (positive * positive).astype(BF16)
+            grad_down[...] = lax.dot_general(
+                hidden, cot_all[...].reshape(tokens, block), TN, preferred_element_type=F32)
+        finish(m - 1, order[m - 1])
+    finish(nf - 1, order[nf - 1])
+    collect(1, in_all)
+    grad_up[...] = lax.dot_general(
+        in_all[...].reshape(tokens, block), pg[...].reshape(tokens, width), TN, preferred_element_type=F32)
+
+    for off in range(1, nf):
+        g = lax.rem(f + nf - off, nf)
+        copy(zt_out.at[0], share.at[t, g], zt_s.at[off], zt_r.at[off], fs=g).wait_recv()
+    for i in range(1, half):
+        start(copy(share.at[t], share.at[t], fa_s.at[i], fa_r.at[i], tp=peer(i)))
+    start(copy(share.at[t], share.at[t], fd_s.at[0], fd_r.at[0], tp=partner))
+    for i in range(1, half):
+        at = share.at[source(i)]
+        copy(at, at, fa_s.at[i], fa_r.at[i], tp=source(i)).wait_recv()
+        start(copy(at, at, fd_s.at[i], fd_r.at[i], tp=partner))
+    for i in range(half):
+        at = share.at[lax.rem(partner + nt - 2 * i, nt)]
+        copy(at, at, fd_s.at[i], fd_r.at[i], tp=partner).wait_recv()
+    grad_input[...] = jnp.concatenate(
+        [share[:, g].reshape(rows, block) for g in range(nf)], axis=1)
+
+    for cond, desc in sent:
+        if cond is None:
+            desc.wait_send()
+        else:
+            pl.when(cond)(desc.wait_send)
+
+
+def in_kernel(nf, nt, inputs, pre_act, cotangent, w_up, w_down):
+    rows, width = pre_act.shape
+    block = w_up.shape[0]
+    part, half, pieces = rows // nt, nt // 2, 2
+    vmem = pl.BlockSpec(memory_space=pltpu.VMEM)
+    dma = pltpu.SemaphoreType.DMA
+    return pl.pallas_call(
+        functools.partial(kernel, nf, nt, pieces),
+        out_shape=(
+            jax.ShapeDtypeStruct((rows, nf * block), BF16),
+            jax.ShapeDtypeStruct((block, width), F32),
+            jax.ShapeDtypeStruct((width, block), F32),
+        ),
+        in_specs=[vmem] * 5,
+        out_specs=(vmem,) * 3,
+        scratch_shapes=[
+            pltpu.VMEM((nf, nt, part, block), BF16),
+            pltpu.VMEM((nf, nt, part, block), BF16),
+            pltpu.VMEM((nf, nt, part, block), BF16),
+            pltpu.VMEM((nf, nt, part, block), BF16),
+            pltpu.VMEM((nf, rows, width), BF16),
+            pltpu.VMEM((nf, rows, width), BF16),
+            pltpu.VMEM((nf, rows, width), F32),
+            pltpu.VMEM((2, nf, rows, width), BF16),
+            pltpu.VMEM((2, nf, rows, width), BF16),
+            pltpu.VMEM((nf, half, part, block), BF16),
+            pltpu.VMEM((nf, half, part, block), BF16),
+            pltpu.VMEM((nf, half, part, block), BF16),
+            pltpu.VMEM((nf, half, part, block), BF16),
+            pltpu.VMEM((nf, half, part, block), BF16),
+            pltpu.VMEM((nf, part, block), BF16),
+            pltpu.VMEM((nt, nf, part, block), BF16),
+            dma((2, nf)), dma((2, nf)),
+            dma((2, nf, half)), dma((2, nf, half)),
+            dma((2, nf, half)), dma((2, nf, half)),
+            dma((2, nf, pieces)), dma((2, nf, pieces)),
+            dma((2, 2, nf, pieces)), dma((2, 2, nf, pieces)),
+            dma((nf,)), dma((nf,)),
+            dma((nf, half)), dma((nf, half)),
+            dma((nf,)), dma((nf,)),
+            dma((half,)), dma((half,)),
+            dma((half,)), dma((half,)),
+        ],
+        compiler_params=pltpu.CompilerParams(
+            collective_id=0, has_side_effects=True, vmem_limit_bytes=60 * 1024 * 1024),
+    )(inputs, pre_act, cotangent, w_up, w_down)
 
 
 def on_device(inputs, pre_act, cotangent, w_up, w_down):
@@ -55,6 +345,14 @@
 def solution(mesh):
     in_specs = (P("fs", None), P("fs", "tp"), P("fs", None), P("fs", "tp"), P("tp", "fs"))
     out_specs = (P("fs", None), P("fs", "tp"), P("tp", "fs"))
+    nf, nt = mesh.shape["fs"], mesh.shape["tp"]
+
+    def body(inputs, pre_act, cotangent, w_up, w_down):
+        rows = pre_act.shape[0]
+        if nt % 2 == 0 and nt >= 4 and nf >= 2 and rows % (16 * nt) == 0:
+            return in_kernel(nf, nt, inputs, pre_act, cotangent, w_up, w_down)
+        return on_device(inputs, pre_act, cotangent, w_up, w_down)
+
     return jax.shard_map(
-        on_device, mesh=mesh, in_specs=in_specs, out_specs=out_specs, check_vma=False
+        body, mesh=mesh, in_specs=in_specs, out_specs=out_specs, check_vma=False
     )

time: 241 us -> 150 us (0.62)
  waiting for transfers between devices: 194 us -> 0 us
  Pallas kernels: 0 us -> 138 us
  between operations: 13.8 us -> 0.65 us
  blocking collectives: 10.9 us -> 0 us
  matrix products: 8.52 us -> 0 us
    pallas_call x0 -> x1, Pallas kernels: none -> 138 us  [in_kernel(): pl.pallas_call(functools.partial(kernel, nf, nt, pieces), out_shape=(jax....]
    all_gather x2 -> x0, waiting for transfers between devices: 87.6 us -> none  [the longest x1 44.5 us: on_device(): lax.all_gather(w_down, 'fs', axis=1, tiled=True)]
    unnamed x7 -> x0, waiting for transfers between devices: 70.4 us -> none
    reduce_scatter x1 -> x0, waiting for transfers between devices: 35.9 us -> none  [on_device(): lax.psum_scatter(partial_sum, 'tp', scatter_dimension=0, tiled=True)]
    all_gather x1 -> x0, blocking collectives: 10.9 us -> none  [on_device(): grad_input = lax.all_gather(shares, 'tp', axis=0, tiled=True)]
    dot_general x4 -> x0, matrix products: 8.52 us -> none  [the longest x1 3.32 us: on_device(): lax.dot_general(pre_grad, lax.all_gather(w_up, 'fs', axis=0, tiled=True),...]
    unnamed x11, local copies, waits for them, and re-layouts: 12 us -> 8.11 us
  transfers between devices with their start and end apart: 5 -> 0, of which waited for: 5 -> 0; matrix products, arithmetic and copies ran while one was open for 7% -> 0% of each run, Pallas kernels for 0% -> 0%
where the time goes in v1:
time: 150 us; the launch traced here: 149 us
  Pallas kernels  138 us (92%)
  local copies, waits for them, and re-layouts  10.5 us (7%)
    pallas_call x1, Pallas kernels, in_kernel(): pl.pallas_call(functools.partial(kernel, nf, nt, pieces), out_shape=(jax....  138 us
    unnamed x11, local copies, waits for them, and re-layouts  8.11 us

profile of v1, /device:TPU:0, one launch (start us, length us, event | category | flops | bytes accessed | tf_op | source)
XLA Modules:
  0.0 149.4 jit_solution(7805149231756569801)
XLA Ops:
  0.6 1.8 %copy.9.pre_act = bf16[256,504]{1,0:T(8,128)(2,1)} copy(bf16[256,504]{0,1:T(8,128)(2,1)} %param.6) | data formatting | bytes 516096 | tf_op args[1]
  2.4 0.0 copy-start
  2.4 2.3 %copy.8.inputs = bf16[256,2016]{1,0:T(8,128)(2,1)} copy(bf16[256,2016]{0,1:T(8,128)(2,1)} %param.5) | data formatting | bytes 2064384 | tf_op args[0]
  4.8 0.0 copy-done
  4.8 1.4 copy.10.cotangent
  6.2 138.2 %shard_map.76 = (bf16[256,2016]{1,0:T(8,128)(2,1)}, f32[504,504]{1,0:T(8,128)}, f32[504,504]{1,0:T(8,128)}) custom-call(bf16[256,2016]{1,0:T(8,128)(2,1)} %copy.8.inputs, bf16[256,504]{1,0:T(8,128)(2,1)} %copy.9.pre_act, bf16[256,2016]{1,0:T(8,128)(2,1)} %copy.10.cotangent, bf16[504,504]{1,0:T(8,128)(2,1)} %w_up.1, bf16[504,504]{1,0:T(8,128)(2,1)} %w_down.1), custom_call_target="tpu_custom_call" | custom-call | tf_op jit(solution)/shard_map/pallas_call | solution.py:255
  144.4 0.0 copy-start.2
  144.4 2.4 %copy.11 = bf16[256,2016]{0,1:T(8,128)(2,1)} copy(bf16[256,2016]{1,0:T(8,128)(2,1)} %get-tuple-element.3) | data formatting | bytes 2064384 | tf_op jit(solution)/shard_map/pallas_call | solution.py:255
  146.8 0.0 copy-done.2
  146.8 0.0 copy-start.1
  146.8 1.0 copy.14
  147.8 0.6 copy-done.1
  148.4 1.0 copy.15
Async XLA Ops:
  2.4 2.3 %copy-start = (bf16[256,2016]{0,1:T(8,128)(2,1)S(1)}, bf16[256,2016]{0,1:T(8,128)(2,1)}, u32[]{:S(2)}) copy-start(bf16[256,2016]{0,1:T(8,128)(2,1)} %param.7) | copy-start | bytes 3096580
  144.4 2.4 %copy-start.2 = (f32[504,504]{1,0:T(8,128)S(1)}, f32[504,504]{1,0:T(8,128)}, u32[]{:S(2)}) copy-start(f32[504,504]{1,0:T(8,128)} %get-tuple-element.10) | copy-start | bytes 3048196
  146.8 1.6 %copy-start.1 = (f32[504,504]{1,0:T(8,128)S(1)}, f32[504,504]{1,0:T(8,128)}, u32[]{:S(2)}) copy-start(f32[504,504]{1,0:T(8,128)} %get-tuple-element.11) | copy-start | bytes 3048196

commit v2 on v1

v2 whole, which is shorter than its diff:
```python
import functools

import jax
import jax.numpy as jnp
from jax import lax
from jax.experimental import pallas as pl
from jax.experimental.pallas import tpu as pltpu
from jax.sharding import PartitionSpec as P

MESH = pl.DeviceIdType.MESH
F32 = jnp.float32
BF16 = jnp.bfloat16
NT = (((1,), (1,)), ((), ()))
NN = (((1,), (0,)), ((), ()))


PIECES = 4


def chunk_of(block, nt):
    return -(-block // (16 * nt)) * 16


def pieces_of(extent, size):
    return [(at, min(size, extent - at)) for at in range(0, extent, size)]


def kernel(nf, nt, size, inputs, pre_act, cotangent, w_up_in, w_down_in, grad_input, grad_up, grad_down,
           cot_split, in_split, cot_all, in_all, pa, pg, hg, w_up, w_down, up_acc, down_acc,
           rs_out, rs_in, px_out, px_in, keep, xy_out, xy_in, zt_out, share,
           a2a_s, a2a_r, ring_s, ring_r, pair_s, pair_r, rs_s, rs_r, ag_s, ag_r,
           px_s, px_r, xy_s, xy_r, zt_s, zt_r, fa_s, fa_r, fd_s, fd_r, load_s):
    f, t = lax.axis_index("fs"), lax.axis_index("tp")
    half = nt // 2
    width, rows = pre_act.shape
    block = w_up.shape[0]
    chunk = cot_all.shape[1] // nt
    cuts = pieces_of(width, size)
    odd = lax.rem(t, 2)
    partner = t + 1 - 2 * odd
    sent = []

    def mine_at(ref, g, c):
        return ref.at[g, pl.ds(pl.multiple_of(c * chunk, chunk), chunk)]

    def copy(src, dst, ssem, rsem, fs=None, tp=None):
        return pltpu.make_async_remote_copy(
            src_ref=src, dst_ref=dst, send_sem=ssem, recv_sem=rsem,
            device_id=(f if fs is None else fs, t if tp is None else tp), device_id_type=MESH,
        )

    def start(desc, cond=None):
        sent.append((cond, desc))
        if cond is None:
            desc.start()
        else:
            pl.when(cond)(desc.start)

    def peer(i):
        return lax.rem(t + 2 * i, nt)

    def source(i):
        return lax.rem(t + nt - 2 * i, nt)

    barrier = pltpu.get_barrier_semaphore()
    for off in range(1, nf):
        pl.semaphore_signal(barrier, inc=1, device_id=(lax.rem(f + off, nf), t), device_id_type=MESH)
    for i in range(1, half):
        pl.semaphore_signal(barrier, inc=1, device_id=(f, peer(i)), device_id_type=MESH)
    pl.semaphore_signal(barrier, inc=1, device_id=(f, partner), device_id_type=MESH)

    loads = []

    def load(src, dst):
        desc = pltpu.make_async_copy(src, dst, load_s.at[len(loads)])
        desc.start()
        loads.append(desc)
        return desc

    def split(src, dst, whole):
        out = [load(src.at[pl.ds(g * block, block)], dst.at[g, pl.ds(0, block)]) for g in range(nf)]
        own = load(src.at[pl.ds(pl.multiple_of(f * block, 8), block)], whole.at[f, pl.ds(0, block)])
        return out, own

    cot_blocks, cot_own = split(cotangent, cot_split, cot_all)
    pa_own = load(pre_act, pa.at[f])
    in_blocks, in_own = split(inputs, in_split, in_all)
    w_down_load = load(w_down_in, w_down)
    w_up_load = load(w_up_in, w_up)
    for desc in cot_blocks:
        desc.wait()
    pl.semaphore_wait(barrier, nf - 1 + half)

    def exchange(n, src, dst):
        for off in range(nf - 1, 0, -1):
            g = lax.rem(f + off, nf)
            start(copy(mine_at(src, g, t), mine_at(dst, f, t), a2a_s.at[n, off], a2a_r.at[n, off], fs=g))

    def spread(n, src, dst):
        for off in range(1, nf):
            g = lax.rem(f + nf - off, nf)
            copy(mine_at(src, g, t), mine_at(dst, g, t), a2a_s.at[n, off], a2a_r.at[n, off], fs=g).wait_recv()
            for i in range(1, half):
                start(copy(mine_at(dst, g, t), mine_at(dst, g, t), ring_s.at[n, off, i], ring_r.at[n, off, i], tp=peer(i)))
            start(copy(mine_at(dst, g, t), mine_at(dst, g, t), pair_s.at[n, off, 0], pair_r.at[n, off, 0], tp=partner))

    def relay(n, dst):
        for off in range(1, nf):
            g = lax.rem(f + nf - off, nf)
            for i in range(1, half):
                at = mine_at(dst, g, source(i))
                copy(at, at, ring_s.at[n, off, i], ring_r.at[n, off, i], tp=source(i)).wait_recv()
                start(copy(at, at, pair_s.at[n, off, i], pair_r.at[n, off, i], tp=partner))

    def collect(n, dst):
        for off in range(1, nf):
            g = lax.rem(f + nf - off, nf)
            for i in range(half):
                at = mine_at(dst, g, lax.rem(partner + nt - 2 * i, nt))
                copy(at, at, pair_s.at[n, off, i], pair_r.at[n, off, i], tp=partner).wait_recv()

    def nearest(m):
        a = jnp.minimum(f, nf - 1 - f)
        j = (m - 1) // 2
        near = f - 1 - j if m % 2 == 1 else f + 1 + j
        far = jnp.where(f < nf - 1 - f, f + (m - a), f - (m - a))
        return jnp.where(m <= 2 * a, near, far)

    def gather_own(n, buf, s, cut):
        at = buf.at[f, pl.ds(*cut)]
        start(copy(at, at, ag_s.at[n, 0, 0, s], ag_r.at[n, 0, 0, s], fs=jnp.minimum(f + 1, nf - 1)), f < nf - 1)
        start(copy(at, at, ag_s.at[n, 1, 0, s], ag_r.at[n, 1, 0, s], fs=jnp.maximum(f - 1, 0)), f > 0)

    def gather_next(n, buf, m, s, cut):
        g = nearest(m)
        up = g < f
        d = jnp.where(up, 0, 1)
        j = jnp.abs(g - f) - 1
        at = buf.at[g, pl.ds(*cut)]
        copy(at, at, ag_s.at[n, d, j, s], ag_r.at[n, d, j, s], fs=jnp.where(up, f - 1, f + 1)).wait_recv()
        to = jnp.where(up, f + 1, f - 1)
        cond = jnp.logical_and(to >= 0, to < nf)
        to = jnp.clip(to, 0, nf - 1)
        k = jnp.minimum(j + 1, nf - 1)
        start(copy(at, at, ag_s.at[n, d, k, s], ag_r.at[n, d, k, s], fs=to), cond)

    exchange(0, cot_split, cot_all)
    pa_own.wait()
    for desc in in_blocks:
        desc.wait()
    spread(0, cot_split, cot_all)
    gather_own(0, pa, 0, (0, width))
    exchange(1, in_split, in_all)
    cot_own.wait()
    in_own.wait()
    w_down_load.wait()
    w_up_load.wait()
    relay(0, cot_all)
    collect(0, cot_all)

    for g in range(nf):
        hg[g] = lax.dot_general(w_down[...], cot_all[g, :block], NN, preferred_element_type=F32)

    def reduce_copy(s, d, g, fs):
        at = pl.ds(*cuts[s])
        return copy(rs_out.at[d, g, at], rs_in.at[d, g, at], rs_s.at[d, g, s], rs_r.at[d, g, s], fs=fs)

    low = f < nf - 1 - f

    def reduce_pass(s, near, k):
        at = pl.ds(*cuts[s])
        up = low if near else jnp.logical_not(low)
        d = jnp.where(up, 0, 1)
        g = jnp.where(up, nf - 1 - k, k)
        to = jnp.clip(jnp.where(up, f + 1, f - 1), 0, nf - 1)
        back = jnp.clip(jnp.where(up, f - 1, f + 1), 0, nf - 1)
        passes = jnp.where(up, g - f, f - g) > 0
        middle = jnp.where(up, f, nf - 1 - f) > 0

        @pl.when(jnp.logical_and(passes, middle))
        def _():
            reduce_copy(s, d, g, back).wait_recv()
            rs_out[d, g, at] = (hg[g, at] + rs_in[d, g, at].astype(F32)).astype(BF16)

        @pl.when(jnp.logical_and(passes, jnp.logical_not(middle)))
        def _():
            rs_out[d, g, at] = hg[g, at].astype(BF16)

        start(reduce_copy(s, d, g, to), passes)

    def reduce_end(s):
        at = pl.ds(*cuts[s])
        for d, there in ((0, f > 0), (1, f < nf - 1)):
            @pl.when(there)
            def _():
                back = jnp.maximum(f - 1, 0) if d == 0 else jnp.minimum(f + 1, nf - 1)
                reduce_copy(s, d, f, back).wait_recv()
                hg[f, at] = hg[f, at] + rs_in[d, f, at].astype(F32)
        positive = jnp.maximum(pa[f, at].astype(F32), 0.0)
        pg[f, at] = (2.0 * positive * hg[f, at]).astype(BF16)
        gather_own(1, pg, s, cuts[s])

    count = len(cuts)
    for s in range(count + 2):
        if s < count:
            for k in range(nf - 1):
                reduce_pass(s, True, k)
        if 1 <= s <= count:
            for k in range(nf - 1):
                reduce_pass(s - 1, False, k)
        if s == 0:
            spread(1, in_split, in_all)
        if s == 1:
            gather_next(0, pa, 1, 0, (0, width))
            relay(1, in_all)
        if s == count and nf > 2:
            gather_next(0, pa, 2, 0, (0, width))
        if s >= 2:
            reduce_end(s - 2)
    for m in range(3, nf):
        gather_next(0, pa, m, 0, (0, width))
    collect(1, in_all)

    def term(step, g):
        value = lax.dot_general(w_up[...], pg[g], NN, preferred_element_type=F32).astype(BF16)
        spare = nt * chunk - block
        if spare:
            value = jnp.concatenate([value, jnp.zeros((spare, rows), BF16)], axis=0)
        value = value.reshape(half, 2, chunk, rows)

        @pl.when(odd == 0)
        def _():
            keep[step] = value[:, 0]
            px_out[step] = value[:, 1]

        @pl.when(odd == 1)
        def _():
            keep[step] = value[:, 1]
            px_out[step] = value[:, 0]

        start(copy(px_out.at[step], px_in.at[step], px_s.at[step], px_r.at[step], tp=partner))
        value = lax.dot_general(in_all[g, :block], pg[g], NT, preferred_element_type=F32)
        up_acc[...] = value if step == 0 else up_acc[...] + value

    def pair_sum(step):
        copy(px_out.at[step], px_in.at[step], px_s.at[step], px_r.at[step], tp=partner).wait_recv()
        xy_out[step] = (keep[step].astype(F32) + px_in[step].astype(F32)).astype(BF16)
        for i in range(1, half):
            start(copy(xy_out.at[step, lax.rem(t // 2 + i, half)], xy_in.at[step, i],
                       xy_s.at[step, i], xy_r.at[step, i], tp=peer(i)))

    def finish(step, g):
        mine = t // 2
        total = keep[step, mine].astype(F32) + px_in[step, mine].astype(F32)
        for i in range(1, half):
            copy(xy_in.at[step, i], xy_in.at[step, i], xy_s.at[step, i], xy_r.at[step, i], tp=source(i)).wait_recv()
            total = total + xy_in[step, i].astype(F32)
        if step == 0:
            share[f, pl.ds(pl.multiple_of(t * chunk, chunk), chunk)] = total.astype(BF16)
        else:
            zt_out[step] = total.astype(BF16)
            off = lax.rem(g - f + nf, nf)
            start(copy(zt_out.at[step], mine_at(share, f, t), zt_s.at[off], zt_r.at[off], fs=g))

    order = [f] + [nearest(m) for m in range(1, nf)]
    term(0, f)
    pair_sum(0)
    for m in range(1, nf):
        for s in range(len(cuts)):
            gather_next(1, pg, m, s, cuts[s])
        term(m, order[m])
        pair_sum(m)
        finish(m - 1, order[m - 1])
    up_store = load(up_acc, grad_up)
    for g in range(nf):
        positive = jnp.maximum(pa[g].astype(F32), 0.0)
        hidden = (positive * positive).astype(BF16)
        value = lax.dot_general(hidden, cot_all[g, :block], NT, preferred_element_type=F32)
        down_acc[...] = value if g == 0 else down_acc[...] + value
    down_store = load(down_acc, grad_down)
    finish(nf - 1, order[nf - 1])

    def stripe(c):
        return share.at[:, pl.ds(pl.multiple_of(c * chunk, chunk), chunk)]

    for off in range(1, nf):
        g = lax.rem(f + nf - off, nf)
        copy(zt_out.at[0], mine_at(share, g, t), zt_s.at[off], zt_r.at[off], fs=g).wait_recv()
    for i in range(1, half):
        start(copy(stripe(t), stripe(t), fa_s.at[i], fa_r.at[i], tp=peer(i)))
    start(copy(stripe(t), stripe(t), fd_s.at[0], fd_r.at[0], tp=partner))
    for i in range(1, half):
        at = stripe(source(i))
        copy(at, at, fa_s.at[i], fa_r.at[i], tp=source(i)).wait_recv()
        start(copy(at, at, fd_s.at[i], fd_r.at[i], tp=partner))
    for i in range(half):
        at = stripe(lax.rem(partner + nt - 2 * i, nt))
        copy(at, at, fd_s.at[i], fd_r.at[i], tp=partner).wait_recv()
    stores = [
        load(share.at[g, pl.ds(0, block)], grad_input.at[pl.ds(g * block, block)]) for g in range(nf)
    ]
    for desc in stores + [down_store, up_store]:
        desc.wait()

    for cond, desc in sent:
        if cond is None:
            desc.wait_send()
        else:
            pl.when(cond)(desc.wait_send)


def in_kernel(nf, nt, inputs, pre_act, cotangent, w_up, w_down):
    rows, width = pre_act.shape
    block = w_up.shape[0]
    half, chunk = nt // 2, chunk_of(block, nt)
    tall = nt * chunk
    size = -(-width // (16 * PIECES)) * 16
    pieces = len(pieces_of(width, size))
    hbm = pl.BlockSpec(memory_space=pl.ANY)
    dma = pltpu.SemaphoreType.DMA
    grad_input, grad_up, grad_down = pl.pallas_call(
        functools.partial(kernel, nf, nt, size),
        out_shape=(
            jax.ShapeDtypeStruct((nf * block, rows), BF16),
            jax.ShapeDtypeStruct((block, width), F32),
            jax.ShapeDtypeStruct((width, block), F32),
        ),
        in_specs=[hbm] * 5,
        out_specs=(hbm,) * 3,
        scratch_shapes=[
            pltpu.VMEM((nf, tall, rows), BF16),
            pltpu.VMEM((nf, tall, rows), BF16),
            pltpu.VMEM((nf, tall, rows), BF16),
            pltpu.VMEM((nf, tall, rows), BF16),
            pltpu.VMEM((nf, width, rows), BF16),
            pltpu.VMEM((nf, width, rows), BF16),
            pltpu.VMEM((nf, width, rows), F32),
            pltpu.VMEM((block, width), BF16),
            pltpu.VMEM((width, block), BF16),
            pltpu.VMEM((block, width), F32),
            pltpu.VMEM((width, block), F32),
            pltpu.VMEM((2, nf, width, rows), BF16),
            pltpu.VMEM((2, nf, width, rows), BF16),
            pltpu.VMEM((nf, half, chunk, rows), BF16),
            pltpu.VMEM((nf, half, chunk, rows), BF16),
            pltpu.VMEM((nf, half, chunk, rows), BF16),
            pltpu.VMEM((nf, half, chunk, rows), BF16),
            pltpu.VMEM((nf, half, chunk, rows), BF16),
            pltpu.VMEM((nf, chunk, rows), BF16),
            pltpu.VMEM((nf, tall, rows), BF16),
            dma((2, nf)), dma((2, nf)),
            dma((2, nf, half)), dma((2, nf, half)),
            dma((2, nf, half)), dma((2, nf, half)),
            dma((2, nf, pieces)), dma((2, nf, pieces)),
            dma((2, 2, nf, pieces)), dma((2, 2, nf, pieces)),
            dma((nf,)), dma((nf,)),
            dma((nf, half)), dma((nf, half)),
            dma((nf,)), dma((nf,)),
            dma((half,)), dma((half,)),
            dma((half,)), dma((half,)),
            dma((3 * nf + 7,)),
        ],
        compiler_params=pltpu.CompilerParams(
            collective_id=0, has_side_effects=True, vmem_limit_bytes=60 * 1024 * 1024),
    )(inputs.T, pre_act.T, cotangent.T, w_up, w_down)
    return grad_input.T, grad_up, grad_down


def on_device(inputs, pre_act, cotangent, w_up, w_down):
    positive = jnp.maximum(pre_act.astype(jnp.float32), 0.0)
    hidden = (positive * positive).astype(jnp.bfloat16)
    columns = cotangent
    hidden_grad = lax.dot_general(
        columns,
        lax.all_gather(w_down, "fs", axis=1, tiled=True),
        (((1,), (1,)), ((), ())),
        preferred_element_type=jnp.float32,
    )
    pre_grad = (2.0 * positive * hidden_grad).astype(jnp.bfloat16)
    columns = inputs
    grad_up = lax.psum_scatter(
        lax.dot_general(
            columns, pre_grad, (((0,), (0,)), ((), ())), preferred_element_type=jnp.float32
        ).astype(jnp.bfloat16),
        "fs",
        scatter_dimension=0,
        tiled=True,
    ).astype(jnp.float32)
    columns = cotangent
    grad_down = (
        lax.psum_scatter(
            lax.dot_general(
                columns, hidden, (((0,), (0,)), ((), ())), preferred_element_type=jnp.float32
            ).astype(jnp.bfloat16),
            "fs",
            scatter_dimension=0,
            tiled=True,
        )
        .astype(jnp.float32)
        .T
    )
    partial_sum = lax.dot_general(
        pre_grad,
        lax.all_gather(w_up, "fs", axis=0, tiled=True),
        (((1,), (1,)), ((), ())),
        preferred_element_type=jnp.float32,
    ).astype(jnp.bfloat16)
    shares = (
        lax.psum_scatter(partial_sum, "tp", scatter_dimension=0, tiled=True)
        .astype(jnp.float32)
        .astype(jnp.bfloat16)
    )
    grad_input = lax.all_gather(shares, "tp", axis=0, tiled=True)
    return (grad_input, grad_up, grad_down)


def solution(mesh):
    in_specs = (P("fs", None), P("fs", "tp"), P("fs", None), P("fs", "tp"), P("tp", "fs"))
    out_specs = (P("fs", None), P("fs", "tp"), P("tp", "fs"))
    nf, nt = mesh.shape["fs"], mesh.shape["tp"]

    def body(inputs, pre_act, cotangent, w_up, w_down):
        rows, width = pre_act.shape
        block = w_up.shape[0]
        tiles = rows % 128 == 0 and width % 8 == 0 and block % 8 == 0
        if tiles and nt % 2 == 0 and nt >= 4 and nf >= 2 and 8 * chunk_of(block, nt) * nt <= 9 * block:
            return in_kernel(nf, nt, inputs, pre_act, cotangent, w_up, w_down)
        return on_device(inputs, pre_act, cotangent, w_up, w_down)

    return jax.shard_map(
        body, mesh=mesh, in_specs=in_specs, out_specs=out_specs, check_vma=False
    )
```

time: 150 us -> 93.2 us (0.62)
  Pallas kernels: 138 us -> 86.3 us
  local copies, waits for them, and re-layouts: 10.5 us -> 4.89 us
    pallas_call x1, Pallas kernels: 138 us -> 86.3 us  [in_kernel(): pl.pallas_call(functools.partial(kernel, nf, nt, size), out_shape=(jax.Sh...]
    unnamed x11 -> x7, local copies, waits for them, and re-layouts: 8.11 us -> 4.89 us
    pallas_call x1 -> x0, local copies, waits for them, and re-layouts: 2.38 us -> none  [in_kernel(): pl.pallas_call(functools.partial(kernel, nf, nt, pieces), out_shape=(jax....]
where the time goes in v2:
time: 93.2 us; the launch traced here: 91.8 us
  Pallas kernels  86.3 us (93%)
  local copies, waits for them, and re-layouts  4.89 us (5%)
    pallas_call x1, Pallas kernels, in_kernel(): pl.pallas_call(functools.partial(kernel, nf, nt, size), out_shape=(jax.Sh...  86.3 us
    unnamed x7, local copies, waits for them, and re-layouts  4.89 us

profile of v2, /device:TPU:0, one launch (start us, length us, event | category | flops | bytes accessed | tf_op | source)
XLA Modules:
  0.0 91.8 jit_solution(13648549709565471174)
XLA Ops:
  0.6 86.3 %shard_map.76 = (bf16[2016,256]{1,0:T(8,128)(2,1)}, f32[504,504]{1,0:T(8,128)}, f32[504,504]{1,0:T(8,128)}) custom-call(bf16[2016,256]{1,0:T(8,128)(2,1)} %bitcast.4, bf16[504,256]{1,0:T(8,128)(2,1)} %bitcast.7, bf16[2016,256]{1,0:T(8,128)(2,1)} %bitcast.5, bf16[504,504]{1,0:T(8,128)(2,1)} %w_up_in.1, bf16[504,504]{1,0:T(8,128)(2,1)} %w_down_in.1), custom_call_target="tpu_custom_call" | custom-call | tf_op jit(solution)/shard_map/pallas_call | solution.py:321
  87.0 0.0 copy-start.1
  87.0 2.3 %copy.11 = bf16[256,2016]{0,1:T(8,128)(2,1)} copy(bf16[256,2016]{0,1:T(8,128)(2,1)} %bitcast.6) | data formatting | bytes 2064384
  89.3 0.0 copy-done.1
  89.3 0.0 copy-start
  89.3 1.0 %copy.12 = f32[504,504]{1,0:T(8,128)} copy(f32[504,504]{1,0:T(8,128)S(1)} %copy-done.1) | data formatting | bytes 2032128
  90.3 0.6 copy-done
  90.9 1.0 %copy.13 = f32[504,504]{1,0:T(8,128)} copy(f32[504,504]{1,0:T(8,128)S(1)} %copy-done) | data formatting | bytes 2032128
Async XLA Ops:
  87.0 2.3 %copy-start.1 = (f32[504,504]{1,0:T(8,128)S(1)}, f32[504,504]{1,0:T(8,128)}, u32[]{:S(2)}) copy-start(f32[504,504]{1,0:T(8,128)} %get-tuple-element.13) | copy-start | bytes 3048196
  89.3 1.6 %copy-start = (f32[504,504]{1,0:T(8,128)S(1)}, f32[504,504]{1,0:T(8,128)}, u32[]{:S(2)}) copy-start(f32[504,504]{1,0:T(8,128)} %get-tuple-element.14) | copy-start | bytes 3048196
